TPU v7x, 32 devices: a whole 2x2x4 slice. The times are simulated.
32 devices in a mesh: sp: 4 (over y, x), dp: 8 (over z, core).
Axes of the slice: x: 2, y: 2, z: 4, core: 2. Of those that a mesh axis runs over, the one named last changes fastest.
Arguments:
- tokens: bfloat16 [8, 768, 4096], P('dp', 'sp'), may hold values from -30 to 30
- query_weight: bfloat16 [4096, 512], P('dp', 'sp'), may hold values from -0.09375 to 0.09375
- key_weight: bfloat16 [4096, 512], P('dp', 'sp'), may hold values from -0.09375 to 0.09375
- value_weight: bfloat16 [4096, 512], P('dp', 'sp'), may hold values from -0.09375 to 0.09375
- cum_gate: float32 [8, 4, 768], P('dp', 'sp'), may hold values from -3072 to 0, as said below
Outputs:
- attended: bfloat16 [8, 768, 512], P('dp', 'sp')
Inputs may be any that keep to these rules, and one draw needn't show every extreme that they name: `cum_gate`: never rising along positions; the first position holds one step's log gate.
All inputs are finite; a program needn't handle non-finite values.
Results may differ from a plain program's by a relative error of at most 0.0076.
The roundings to bfloat16 on the way count: a program that leaves them out, or rounds other values in their place, can miss the bound.
Values may be sent and summed in bfloat16 or wider, within the bound.
A program may use at most 128 MiB of HBM per device.

v0:
```python
import jax
import jax.numpy as jnp
from jax import lax
from jax.sharding import PartitionSpec as P

block_rows = 512


def attend(queries, keys, values, gates):
    length = queries.shape[0]
    scale = queries.shape[1] ** (-0.5)
    pieces = []
    for start in range(0, length, block_rows):
        finish = min(start + block_rows, length)
        scores = (
            jnp.dot(queries[start:finish], keys[:finish].T, preferred_element_type=jnp.float32)
            * scale
        )
        scores = scores + gates[start:finish, None] - gates[None, :finish]
        rows_at = start + lax.broadcasted_iota(jnp.int32, scores.shape, 0)
        cols_at = lax.broadcasted_iota(jnp.int32, scores.shape, 1)
        scores = jnp.where(cols_at <= rows_at, scores, -1e30)
        top = jnp.max(scores, axis=1, keepdims=True)
        weights = jnp.exp(scores - top)
        total = jnp.sum(weights, axis=1, keepdims=True)
        summed = jnp.dot(
            weights.astype(jnp.bfloat16), values[:finish], preferred_element_type=jnp.float32
        )
        pieces.append((summed / total).astype(jnp.bfloat16))
    return jnp.concatenate(pieces, axis=0)


def body(tokens, query_weight, key_weight, value_weight, cum_gate):
    width = query_weight.shape[1]
    full_query, full_key, full_value = (
        lax.all_gather(query_weight, "dp", axis=0, tiled=True),
        lax.all_gather(key_weight, "dp", axis=0, tiled=True),
        lax.all_gather(value_weight, "dp", axis=0, tiled=True),
    )
    stacked = jnp.concatenate([full_query, full_key, full_value], axis=1)
    own_rows = tokens[0]
    projected = jnp.dot(
        lax.all_gather(own_rows, "sp", axis=0, tiled=True),
        stacked,
        preferred_element_type=jnp.float32,
    )
    queries = projected[:, :width].astype(jnp.bfloat16)
    keys = projected[:, width : 2 * width].astype(jnp.bfloat16)
    values = projected[:, 2 * width :].astype(jnp.bfloat16)
    head_out = attend(queries, keys, values, cum_gate[0, 0])
    gathered = lax.all_to_all(head_out, "sp", split_axis=0, concat_axis=1, tiled=True)
    return gathered[None]


def solution(mesh):
    in_specs = (
        P("dp", "sp", None),
        P("dp", "sp"),
        P("dp", "sp"),
        P("dp", "sp"),
        P("dp", "sp", None),
    )
    out_specs = P("dp", "sp", None)
    return jax.shard_map(body, mesh=mesh, in_specs=in_specs, out_specs=out_specs, check_vma=False)
```

profile of v0, /device:TPU:0, one launch (start us, length us, event | category | flops | bytes accessed | tf_op | source)
XLA Modules:
  0.0 176.3 jit_solution(13971013935284889980)
XLA Ops:
  6.5 0.0 all-gather.6.cloned.1.call-start
  6.5 0.7 all-gather.6.cloned.1.call-update
  7.3 0.0 all-gather.8.cloned.1.call-start
  7.3 0.7 all-gather.8.cloned.1.call-update
  8.0 0.0 all-gather.10.cloned.1.call-start
  8.1 0.7 all-gather.10.cloned.1.call-update
  8.7 0.0 all-gather.12.cloned.1.call-start
  8.8 0.5 all-gather.12.cloned.1.call-update
  9.3 0.7 reduce
  10.0 0.0 slice-start
  10.0 0.0 slice-start.1
  10.1 23.9 %all-gather.6.cloned.1.call-done = bf16[4096,128]{1,0:T(8,128)(2,1)} async-done(((bf16[512,128]{1,0:T(8,128)(2,1)}), bf16[4096,128]{1,0:T(8,128)(2,1)}) %all-gather.6.cloned.1.call-update) | async-done | bytes 1048592 | tf_op jit(solution)/shard_map/all_gather | solution.py:36
  33.9 23.5 %all-gather.8.cloned.1.call-done = bf16[4096,128]{1,0:T(8,128)(2,1)} async-done(((bf16[512,128]{1,0:T(8,128)(2,1)}), bf16[4096,128]{1,0:T(8,128)(2,1)}) %all-gather.8.cloned.1.call-update) | async-done | bytes 1048592 | tf_op jit(solution)/shard_map/all_gather | solution.py:37
  57.4 23.5 %all-gather.10.cloned.1.call-done = bf16[4096,128]{1,0:T(8,128)(2,1)} async-done(((bf16[512,128]{1,0:T(8,128)(2,1)}), bf16[4096,128]{1,0:T(8,128)(2,1)}) %all-gather.10.cloned.1.call-update) | async-done | bytes 1048592 | tf_op jit(solution)/shard_map/all_gather | solution.py:38
  80.9 71.4 %all-gather.12.cloned.1.call-done = bf16[1,768,4096]{2,1,0:T(8,128)(2,1)} async-done(((bf16[1,192,4096]{2,1,0:T(8,128)(2,1)}), bf16[1,768,4096]{2,1,0:T(8,128)(2,1)}) %all-gather.12.cloned.1.call-update) | async-done | bytes 6291472 | tf_op jit(solution)/shard_map/all_gather | solution.py:43
  152.3 6.4 %fusion.18 = bf16[768,384]{0,1:T(8,128)(2,1)S(1)} fusion(bf16[1,768,4096]{2,1,0:T(8,128)(2,1)} %all-gather.12.cloned.1.call-done, bf16[4096,128]{1,0:T(8,128)(2,1)} %all-gather.10.cloned.1.call-done, bf16[4096,128]{1,0:T(8,128)(2,1)} %all-gather.8.cloned.1.call-done, bf16[4096,128]{1,0:T(8,128)(2,1)} %all-gather.6.cloned.1.call-done), kind=kOutput, calls=%fused_computation.16 | convolution fusion | flops 2425651200 | bytes 10027008 | tf_op jit(solution)/shard_map/dot_general | solution.py:42
  158.7 0.0 slice-done
  158.7 0.4 fusion.40
  159.1 0.3 fusion.27
  159.4 0.3 fusion.24
  159.7 0.0 slice-done.1
  159.8 0.4 fusion.41
  160.1 0.2 fusion.25
  160.3 0.4 fusion.23
  160.7 8.1 %all_to_all.16 = bf16[4,192,128]{2,1,0:T(8,128)(2,1)S(1)} all-to-all(bf16[4,192,128]{2,1,0:T(8,128)(2,1)S(1)} %bitcast.13), channel_id=1, replica_groups=mesh['sp'=4,'dp'=8] {'sp'}, dimensions={0} | all-to-all | bytes 393216 | tf_op jit(solution)/shard_map/all_to_all | solution.py:51
  168.8 0.2 copy.6
  169.0 0.8 broadcast_in_dim.20
  (2 shorter events, 0.0 us)
Async XLA Ops:
  6.5 27.4 %all-gather.6.cloned.1.call-start = ((), (), s32[]{:S(2)}) async-start(), calls=%async_computation.1 | async-start | bytes 1179648 | tf_op jit(solution)/shard_map/all_gather | solution.py:36
  7.3 50.1 %all-gather.8.cloned.1.call-start = ((), (), s32[]{:S(2)}) async-start(), calls=%async_computation.2 | async-start | bytes 1179648 | tf_op jit(solution)/shard_map/all_gather | solution.py:37
  8.0 72.9 %all-gather.10.cloned.1.call-start = ((), (), s32[]{:S(2)}) async-start(), calls=%async_computation.3 | async-start | bytes 1179648 | tf_op jit(solution)/shard_map/all_gather | solution.py:38
  8.7 143.5 %all-gather.12.cloned.1.call-start = ((), (), s32[]{:S(2)}) async-start(), calls=%async_computation.4 | async-start | bytes 7864320 | tf_op jit(solution)/shard_map/all_gather | solution.py:43
  10.0 148.6 %slice-start = ((f32[1,1,768]{2,1,0:T(1,128)}), f32[1,1,256]{2,1,0:T(1,128)S(1)}, s32[]{:S(2)}) async-start(f32[1,1,768]{2,1,0:T(1,128)} %param.9), calls=%async_computation.5 | async-start | bytes 2048 | tf_op jit(solution)/shard_map/slice | solution.py:19
  10.0 149.7 %slice-start.1 = ((f32[1,1,768]{2,1,0:T(1,128)}), f32[1,1,512]{2,1,0:T(1,128)S(1)}, s32[]{:S(2)}) async-start(f32[1,1,768]{2,1,0:T(1,128)} %param.9), calls=%async_computation.6 | async-start | bytes 4096 | tf_op jit(solution)/shard_map/slice | solution.py:19
Sparse Core Ops, SparseCore 0:
  8.9 24.9 all-gather.5
  35.5 21.8 all-gather.7
  59.0 21.8 all-gather.9
  82.6 69.6 all-gather.11
where the time goes:
time: 176 us
  waiting for transfers between devices  145 us (82%)
  between operations  13.2 us (8%)
  blocking collectives  8.09 us (5%)
  matrix products  7.93 us (5%)
    all_gather x1, waiting for transfers between devices, body(): lax.all_gather(own_rows, 'sp', axis=0, tiled=True)  71.4 us
    all_gather x1, waiting for transfers between devices, body(): lax.all_gather(query_weight, 'dp', axis=0, tiled=True)  23.9 us
    all_gather x1, waiting for transfers between devices, body(): lax.all_gather(value_weight, 'dp', axis=0, tiled=True)  23.5 us
    all_gather x1, waiting for transfers between devices, body(): lax.all_gather(key_weight, 'dp', axis=0, tiled=True)  23.5 us
    all_to_all x1, blocking collectives, body(): lax.all_to_all(head_out, 'sp', split_axis=0, concat_axis=1, tiled=True)  8.09 us
    dot_general x1, matrix products, body(): jnp.dot(lax.all_gather(own_rows, 'sp', axis=0, tiled=True), stacked, pref...  6.41 us
  transfers between devices with their start and end apart: 4, of which 4 were waited for; matrix products, arithmetic and copies ran while one was open for 0% of the time, Pallas kernels for 0%

commit v1 on v0

v1 whole, which is shorter than its diff:
```python
import functools
import math

import jax
import jax.numpy as jnp
from jax import lax
from jax.experimental import pallas as pl
from jax.experimental.pallas import tpu as pltpu
from jax.sharding import PartitionSpec as P

MESH = pl.DeviceIdType.MESH
block_rows = 256


def kernel(
    nx, ny, nz, cores,
    tok_hbm, wq_hbm, wk_hbm, wv_hbm, gate_ref, out_ref,
    xbuf, wbuf, qkv, qout, gcol, attn, obuf,
    lsem, xsend, xrecv, wrecv, upsem, downsem, psem, ysem, qsend, qrecv, osend, orecv,
):
    tok, depth = tok_hbm.shape
    head = wq_hbm.shape[1]
    group = nx * tok
    length = ny * group
    s, d = lax.axis_index("sp"), lax.axis_index("dp")
    y, x = s // nx, s % nx
    z, c = d // cores, d % cores

    loads = [
        pltpu.make_async_copy(ref, wbuf.at[y, d, :, pl.ds(i * head, head)], lsem.at[i])
        for i, ref in enumerate((wq_hbm, wk_hbm, wv_hbm))
    ]
    loads.append(pltpu.make_async_copy(tok_hbm, xbuf.at[x], lsem.at[3]))
    for load in loads:
        load.start()

    barrier = pltpu.get_barrier_semaphore()
    for k in range(1, nx * ny):
        pl.semaphore_signal(
            barrier, inc=1, device_id={"sp": (s + k) % (nx * ny)}, device_id_type=MESH
        )
    for k in range(1, nz):
        pl.semaphore_signal(
            barrier, inc=1, device_id={"dp": ((z + k) % nz) * cores + c}, device_id_type=MESH
        )
    if cores > 1:
        pl.semaphore_signal(
            barrier, inc=1, device_id={"dp": z * cores + 1 - c}, device_id_type=MESH
        )
    pl.semaphore_wait(barrier, nx * ny - 1 + nz - 1 + cores - 1)

    def send_tokens(j):
        return pltpu.make_async_remote_copy(
            src_ref=tok_hbm, dst_ref=xbuf.at[x],
            send_sem=xsend.at[j - 1], recv_sem=xrecv.at[x],
            device_id={"sp": y * nx + (x + j) % nx}, device_id_type=MESH,
        )

    for j in range(1, nx):
        send_tokens(j).start()

    def send_block(h, zb, sem, device):
        at = zb * cores + c
        return pltpu.make_async_remote_copy(
            src_ref=wbuf.at[h, at], dst_ref=wbuf.at[h, at],
            send_sem=sem, recv_sem=wrecv.at[h, at],
            device_id=device, device_id_type=MESH,
        )

    def up(zb):
        return send_block(y, zb, upsem.at[zb], {"dp": jnp.minimum(z + 1, nz - 1) * cores + c})

    def down(zb):
        return send_block(y, zb, downsem.at[zb], {"dp": jnp.maximum(z - 1, 0) * cores + c})

    def across(h, zb):
        return send_block(h, zb, psem.at[h, zb], {"dp": z * cores + 1 - c})

    def aside(k, zb):
        return send_block(y, zb, ysem.at[k - 1, zb], {"sp": ((y + k) % ny) * nx + x})

    def arrived(h, at):
        pltpu.make_async_remote_copy(
            src_ref=wbuf.at[h, at], dst_ref=wbuf.at[h, at],
            send_sem=lsem.at[0], recv_sem=wrecv.at[h, at],
            device_id={"sp": (s + 1) % (nx * ny)}, device_id_type=MESH,
        ).wait_recv()

    def spread(zb):
        for k in range(1, ny):
            aside(k, zb).start()
        if cores > 1:
            across(y, zb).start()

    for load in loads[:3]:
        load.wait()

    pl.when(z < nz - 1)(lambda: up(z).start())
    pl.when(z > 0)(lambda: down(z).start())
    spread(z)

    for start in range(0, length, 128):
        row = gate_ref[:, start : start + 128]
        gcol[start : start + 128, :] = jnp.broadcast_to(row, (128, 128)).T

    for t in range(1, nz):

        @pl.when(z - t >= 0)
        def _(t=t):
            arrived(y, (z - t) * cores + c)
            pl.when(z < nz - 1)(lambda: up(z - t).start())
            spread(z - t)

        @pl.when(z + t < nz)
        def _(t=t):
            arrived(y, (z + t) * cores + c)
            pl.when(z > 0)(lambda: down(z + t).start())
            spread(z + t)

    if cores > 1:
        for zb in range(nz):
            arrived(y, zb * cores + 1 - c)

    def project(i, h):
        weights = wbuf[h].reshape(depth, 3 * head)
        return jnp.dot(xbuf[i], weights, preferred_element_type=jnp.float32).astype(jnp.bfloat16)

    def own_rows(i):
        return pl.ds(pl.multiple_of(y * group + i * tok, tok), tok)

    loads[3].wait()
    qkv[own_rows(x), :] = project(x, y)

    def from_side(zb):
        for k in range(1, ny):
            other = (y + ny - k) % ny
            arrived(other, zb * cores + c)
            if cores > 1:
                across(other, zb).start()

    from_side(z)
    for t in range(1, nz):
        pl.when(z - t >= 0)(lambda t=t: from_side(z - t))
        pl.when(z + t < nz)(lambda t=t: from_side(z + t))
    if cores > 1:
        for k in range(1, ny):
            for zb in range(nz):
                arrived((y + k) % ny, zb * cores + 1 - c)

    def send_qkv(k, i):
        return pltpu.make_async_remote_copy(
            src_ref=qout.at[k - 1, i], dst_ref=qkv.at[own_rows(i)],
            send_sem=qsend.at[k - 1, i], recv_sem=qrecv.at[y, i],
            device_id={"sp": ((y + k) % ny) * nx + x}, device_id_type=MESH,
        )

    def swap(i):
        for k in range(1, ny):
            qout[k - 1, i] = project(i, (y + k) % ny)
            send_qkv(k, i).start()

    swap(x)
    for j in range(1, nx):
        i = (x + j) % nx
        pltpu.make_async_remote_copy(
            src_ref=tok_hbm, dst_ref=xbuf.at[i],
            send_sem=xsend.at[j - 1], recv_sem=xrecv.at[i],
            device_id={"sp": (s + 1) % (nx * ny)}, device_id_type=MESH,
        ).wait_recv()
        swap(i)
    for j in range(1, nx):
        i = (x + j) % nx
        qkv[own_rows(i), :] = project(i, y)
    for k in range(1, ny):
        other = (y + k) % ny
        for i in range(nx):
            rows = pl.ds(pl.multiple_of(other * group + i * tok, tok), tok)
            pltpu.make_async_remote_copy(
                src_ref=qout.at[k - 1, i], dst_ref=qkv.at[rows],
                send_sem=qsend.at[k - 1, i], recv_sem=qrecv.at[other, i],
                device_id={"sp": other * nx + x}, device_id_type=MESH,
            ).wait_recv()

    def send_out(to):
        return pltpu.make_async_remote_copy(
            src_ref=attn.at[pl.ds(to * tok, tok)],
            dst_ref=obuf.at[:, pl.ds(pl.multiple_of(s * head, head), head)],
            send_sem=osend.at[to], recv_sem=orecv.at[s],
            device_id={"sp": to}, device_id_type=MESH,
        )

    scale = head ** (-0.5)
    sent = 0
    for start in range(0, length, block_rows):
        finish = min(start + block_rows, length)
        scores = (
            lax.dot_general(
                qkv[start:finish, :head], qkv[:finish, head : 2 * head],
                (((1,), (1,)), ((), ())), preferred_element_type=jnp.float32,
            )
            * scale
        )
        scores = scores + gcol[start:finish, :1] - gate_ref[:, :finish]
        rows_at = start + lax.broadcasted_iota(jnp.int32, scores.shape, 0)
        cols_at = lax.broadcasted_iota(jnp.int32, scores.shape, 1)
        scores = jnp.where(cols_at <= rows_at, scores, -1e30)
        top = jnp.max(scores, axis=1, keepdims=True)
        weights = jnp.exp(scores - top)
        total = jnp.sum(weights, axis=1, keepdims=True)
        summed = jnp.dot(
            weights.astype(jnp.bfloat16), qkv[:finish, 2 * head :],
            preferred_element_type=jnp.float32,
        )
        attn[start:finish, :] = (summed / total).astype(jnp.bfloat16)
        while (sent + 1) * tok <= finish:

            @pl.when(s != sent)
            def _(to=sent):
                send_out(to).start()

            @pl.when(s == sent)
            def _(to=sent):
                obuf[:, pl.ds(pl.multiple_of(s * head, head), head)] = attn[
                    to * tok : (to + 1) * tok, :
                ]

            sent += 1

    for k in range(1, nx * ny):
        source = (s + k) % (nx * ny)
        pltpu.make_async_remote_copy(
            src_ref=attn.at[pl.ds(0, tok)],
            dst_ref=obuf.at[:, pl.ds(pl.multiple_of(source * head, head), head)],
            send_sem=osend.at[source], recv_sem=orecv.at[source],
            device_id={"sp": source}, device_id_type=MESH,
        ).wait_recv()
    out_ref[...] = obuf[...]

    for j in range(1, nx):
        send_tokens(j).wait_send()
    for zb in range(nz):
        pl.when((z < nz - 1) & (zb <= z))(lambda zb=zb: up(zb).wait_send())
        pl.when((z > 0) & (zb >= z))(lambda zb=zb: down(zb).wait_send())
        for k in range(1, ny):
            aside(k, zb).wait_send()
        if cores > 1:
            for h in range(ny):
                across(h, zb).wait_send()
    for k in range(1, ny):
        for i in range(nx):
            send_qkv(k, i).wait_send()
    for to in range(nx * ny):
        pl.when(s != to)(lambda to=to: send_out(to).wait_send())


def body(sp, dp, tokens, query_weight, key_weight, value_weight, cum_gate):
    nx = max(n for n in range(1, math.isqrt(sp) + 1) if sp % n == 0)
    ny = sp // nx
    cores = 2 if dp % 2 == 0 else 1
    nz = dp // cores
    tok, depth = tokens.shape[1:]
    rows, head = query_weight.shape
    length = sp * tok
    dma = pltpu.SemaphoreType.DMA
    anywhere = pl.BlockSpec(memory_space=pl.ANY)
    vmem = pl.BlockSpec(memory_space=pltpu.VMEM)
    out = pl.pallas_call(
        functools.partial(kernel, nx, ny, nz, cores),
        out_shape=jax.ShapeDtypeStruct((tok, sp * head), jnp.bfloat16),
        in_specs=[anywhere] * 4 + [vmem],
        out_specs=vmem,
        scratch_shapes=[
            pltpu.VMEM((nx, tok, depth), jnp.bfloat16),
            pltpu.VMEM((ny, dp, rows, 3 * head), jnp.bfloat16),
            pltpu.VMEM((length, 3 * head), jnp.bfloat16),
            pltpu.VMEM((ny - 1, nx, tok, 3 * head), jnp.bfloat16),
            pltpu.VMEM((length, 128), jnp.float32),
            pltpu.VMEM((length, head), jnp.bfloat16),
            pltpu.VMEM((tok, sp * head), jnp.bfloat16),
            dma((4,)),
            dma((nx - 1,)),
            dma((nx,)),
            dma((ny, dp)),
            dma((nz,)),
            dma((nz,)),
            dma((ny, nz)),
            dma((ny - 1, nz)),
            dma((ny - 1, nx)),
            dma((ny, nx)),
            dma((sp,)),
            dma((sp,)),
        ],
        compiler_params=pltpu.CompilerParams(
            collective_id=0, has_side_effects=True, vmem_limit_bytes=60 * 1024 * 1024
        ),
    )(tokens[0], query_weight, key_weight, value_weight, cum_gate[0])
    return out[None]


def solution(mesh):
    in_specs = (
        P("dp", "sp", None),
        P("dp", "sp"),
        P("dp", "sp"),
        P("dp", "sp"),
        P("dp", "sp", None),
    )
    out_specs = P("dp", "sp", None)
    return jax.shard_map(
        functools.partial(body, mesh.shape["sp"], mesh.shape["dp"]),
        mesh=mesh, in_specs=in_specs, out_specs=out_specs, check_vma=False,
    )
```

time: 176 us -> 59.3 us (0.34)
  waiting for transfers between devices: 145 us -> 0 us
  Pallas kernels: 0 us -> 57.5 us
  between operations: 13.2 us -> 0.01 us
  blocking collectives: 8.09 us -> 0 us
  matrix products: 7.93 us -> 0 us
    all_gather x4 -> x0, waiting for transfers between devices: 142 us -> none  [the longest x1 71.4 us: body(): lax.all_gather(own_rows, 'sp', axis=0, tiled=True)]
    pallas_call x0 -> x1, Pallas kernels: none -> 57.5 us  [body(): pl.pallas_call(functools.partial(kernel, nx, ny, nz, cores), out_shape=ja...]
    all_to_all x1 -> x0, blocking collectives: 8.09 us -> none  [body(): lax.all_to_all(head_out, 'sp', split_axis=0, concat_axis=1, tiled=True)]
    dot_general x5 -> x0, matrix products: 7.93 us -> none  [the longest x1 6.41 us: body(): jnp.dot(lax.all_gather(own_rows, 'sp', axis=0, tiled=True), stacked, pref...]
    unnamed x4 -> x0, waiting for transfers between devices: 2.61 us -> none
  transfers between devices with their start and end apart: 4 -> 0, of which waited for: 4 -> 0; matrix products, arithmetic and copies ran while one was open for 0% -> 0% of each run, Pallas kernels for 0% -> 0%
where the time goes in v1:
time: 59.3 us; the launch traced here: 59.1 us
  Pallas kernels  57.5 us (97%)
  local copies, waits for them, and re-layouts  1.62 us (3%)
    pallas_call x1, Pallas kernels, body(): pl.pallas_call(functools.partial(kernel, nx, ny, nz, cores), out_shape=ja...  57.5 us
    unnamed x1, local copies, waits for them, and re-layouts  1.62 us

profile of v1, /device:TPU:0, one launch (start us, length us, event | category | flops | bytes accessed | tf_op | source)
XLA Modules:
  0.0 59.1 jit_solution(2439438659950136872)
XLA Ops:
  0.0 57.5 %shard_map.55 = bf16[192,512]{1,0:T(8,128)(2,1)} custom-call(bf16[192,4096]{1,0:T(8,128)(2,1)} %bitcast.3, bf16[512,128]{1,0:T(8,128)(2,1)} %wq_hbm.1, bf16[512,128]{1,0:T(8,128)(2,1)} %wk_hbm.1, bf16[512,128]{1,0:T(8,128)(2,1)} %wv_hbm.1, f32[1,768]{1,0:T(1,128)} %bitcast.5), custom_call_target="tpu_custom_call" | custom-call | tf_op jit(solution)/shard_map/pallas_call | solution.py:267
  57.5 1.6 %copy.7 = bf16[1,192,512]{2,1,0:T(8,128)(2,1)} copy(bf16[1,192,512]{2,1,0:T(8,128)(2,1)} %bitcast.4) | data formatting | bytes 393216

commit v2 on v1

--- a/solution.py
+++ b/solution.py
@@ -15,23 +15,31 @@
 def kernel(
     nx, ny, nz, cores,
     tok_hbm, wq_hbm, wk_hbm, wv_hbm, gate_ref, out_ref,
-    xbuf, wbuf, qkv, qout, gcol, attn, obuf,
-    lsem, xsend, xrecv, wrecv, upsem, downsem, psem, ysem, qsend, qrecv, osend, orecv,
+    xbuf, wbuf, acc, qkv, qout, gcol, attn, obuf,
+    lsem, tsem, xsend, xrecv, wrecv, upsem, downsem, upq, downq, psem, pq, ysem, yq,
+    qsend, qrecv, osend, orecv,
 ):
     tok, depth = tok_hbm.shape
-    head = wq_hbm.shape[1]
+    rows, head = wq_hbm.shape
+    early = rows // 4
+    chunk = cores * rows
     group = nx * tok
     length = ny * group
     s, d = lax.axis_index("sp"), lax.axis_index("dp")
     y, x = s // nx, s % nx
     z, c = d // cores, d % cores
 
+    def piece(zb):
+        return tok_hbm.at[:, pl.ds(pl.multiple_of(zb * chunk, chunk), chunk)]
+
     loads = [
         pltpu.make_async_copy(ref, wbuf.at[y, d, :, pl.ds(i * head, head)], lsem.at[i])
         for i, ref in enumerate((wq_hbm, wk_hbm, wv_hbm))
     ]
-    loads.append(pltpu.make_async_copy(tok_hbm, xbuf.at[x], lsem.at[3]))
-    for load in loads:
+    own_loads = [
+        pltpu.make_async_copy(piece(zb), xbuf.at[x, zb], tsem.at[zb]) for zb in range(nz)
+    ]
+    for load in loads + own_loads:
         load.start()
 
     barrier = pltpu.get_barrier_semaphore()
@@ -49,134 +57,191 @@
         )
     pl.semaphore_wait(barrier, nx * ny - 1 + nz - 1 + cores - 1)
 
-    def send_tokens(j):
+    def step(t, act):
+        if t == 0:
+            act(z)
+            return
+        pl.when(z - t >= 0)(lambda: act(z - t))
+        pl.when(z + t < nz)(lambda: act(z + t))
+
+    def send_tokens(j, zb):
         return pltpu.make_async_remote_copy(
-            src_ref=tok_hbm, dst_ref=xbuf.at[x],
-            send_sem=xsend.at[j - 1], recv_sem=xrecv.at[x],
+            src_ref=piece(zb), dst_ref=xbuf.at[x, zb],
+            send_sem=xsend.at[j - 1, zb], recv_sem=xrecv.at[x, zb],
             device_id={"sp": y * nx + (x + j) % nx}, device_id_type=MESH,
         )
 
-    for j in range(1, nx):
-        send_tokens(j).start()
-
-    def send_block(h, zb, sem, device):
+    def view(h, at, part):
+        if part == 0:
+            return wbuf.at[h, at]
+        if part == 1:
+            return wbuf.at[h, at, pl.ds(0, early)]
+        return wbuf.at[h, at, pl.ds(early, rows - early)]
+
+    def send_block(h, zb, part, sem, device):
         at = zb * cores + c
         return pltpu.make_async_remote_copy(
-            src_ref=wbuf.at[h, at], dst_ref=wbuf.at[h, at],
-            send_sem=sem, recv_sem=wrecv.at[h, at],
+            src_ref=view(h, at, part), dst_ref=view(h, at, part),
+            send_sem=sem, recv_sem=wrecv.at[int(part == 1), h, at],
             device_id=device, device_id_type=MESH,
         )
 
+    above = {"dp": jnp.minimum(z + 1, nz - 1) * cores + c}
+    below = {"dp": jnp.maximum(z - 1, 0) * cores + c}
+    beside = {"dp": z * cores + 1 - c}
+
+    def aside(k):
+        return {"sp": ((y + k) % ny) * nx + x}
+
     def up(zb):
-        return send_block(y, zb, upsem.at[zb], {"dp": jnp.minimum(z + 1, nz - 1) * cores + c})
+        return send_block(y, zb, 0, upsem.at[zb], above)
 
     def down(zb):
-        return send_block(y, zb, downsem.at[zb], {"dp": jnp.maximum(z - 1, 0) * cores + c})
-
-    def across(h, zb):
-        return send_block(h, zb, psem.at[h, zb], {"dp": z * cores + 1 - c})
-
-    def aside(k, zb):
-        return send_block(y, zb, ysem.at[k - 1, zb], {"sp": ((y + k) % ny) * nx + x})
-
-    def arrived(h, at):
+        return send_block(y, zb, 0, downsem.at[zb], below)
+
+    def up_early(h, zb):
+        return send_block(h, zb, 1, upq.at[h, zb], above)
+
+    def down_early(h, zb):
+        return send_block(h, zb, 1, downq.at[h, zb], below)
+
+    def across(h, zb, part):
+        return send_block(h, zb, part, (pq if part == 1 else psem).at[h, zb], beside)
+
+    def side_early(k):
+        return send_block(y, z, 1, yq.at[k - 1], aside(k))
+
+    def side_late(k, zb):
+        return send_block(y, zb, 2, ysem.at[k - 1, zb], aside(k))
+
+    def arrived(h, at, part):
         pltpu.make_async_remote_copy(
-            src_ref=wbuf.at[h, at], dst_ref=wbuf.at[h, at],
-            send_sem=lsem.at[0], recv_sem=wrecv.at[h, at],
+            src_ref=view(h, at, part), dst_ref=view(h, at, part),
+            send_sem=lsem.at[0], recv_sem=wrecv.at[int(part == 1), h, at],
             device_id={"sp": (s + 1) % (nx * ny)}, device_id_type=MESH,
         ).wait_recv()
 
+    others = [(y + k) % ny for k in range(1, ny)]
+
+    for load in loads:
+        load.wait()
+
     def spread(zb):
         for k in range(1, ny):
-            aside(k, zb).start()
+            side_late(k, zb).start()
         if cores > 1:
-            across(y, zb).start()
-
-    for load in loads[:3]:
-        load.wait()
-
+            across(y, zb, 0).start()
+
+    for k in range(1, ny):
+        side_early(k).start()
     pl.when(z < nz - 1)(lambda: up(z).start())
     pl.when(z > 0)(lambda: down(z).start())
+    for j in range(1, nx):
+        send_tokens(j, z).start()
     spread(z)
+    for t in range(1, nz):
+        for j in range(1, nx):
+            step(t, lambda zb, j=j: send_tokens(j, zb).start())
 
     for start in range(0, length, 128):
         row = gate_ref[:, start : start + 128]
         gcol[start : start + 128, :] = jnp.broadcast_to(row, (128, 128)).T
-
-    for t in range(1, nz):
-
-        @pl.when(z - t >= 0)
-        def _(t=t):
-            arrived(y, (z - t) * cores + c)
-            pl.when(z < nz - 1)(lambda: up(z - t).start())
-            spread(z - t)
-
-        @pl.when(z + t < nz)
-        def _(t=t):
-            arrived(y, (z + t) * cores + c)
-            pl.when(z > 0)(lambda: down(z + t).start())
-            spread(z + t)
-
-    if cores > 1:
-        for zb in range(nz):
-            arrived(y, zb * cores + 1 - c)
-
-    def project(i, h):
-        weights = wbuf[h].reshape(depth, 3 * head)
-        return jnp.dot(xbuf[i], weights, preferred_element_type=jnp.float32).astype(jnp.bfloat16)
+    acc[...] = jnp.zeros_like(acc)
+
+    def relay(t):
+        def from_below(zb):
+            arrived(y, zb * cores + c, 0)
+            pl.when(z < nz - 1)(lambda: up(zb).start())
+            spread(zb)
+
+        def from_above(zb):
+            arrived(y, zb * cores + c, 0)
+            pl.when(z > 0)(lambda: down(zb).start())
+            spread(zb)
+
+        def hand_on(zb, upward, downward):
+            for h in others:
+                arrived(h, zb * cores + c, 1)
+                if upward:
+                    pl.when(z < nz - 1)(lambda h=h: up_early(h, zb).start())
+                if downward:
+                    pl.when(z > 0)(lambda h=h: down_early(h, zb).start())
+                if cores > 1:
+                    across(h, zb, 1).start()
+
+        if t == 0:
+            hand_on(z, True, True)
+            return
+        pl.when(z - t >= 0)(lambda: from_below(z - t))
+        pl.when(z + t < nz)(lambda: from_above(z + t))
+        pl.when(z - t >= 0)(lambda: hand_on(z - t, True, False))
+        pl.when(z + t < nz)(lambda: hand_on(z + t, False, True))
+
+    def from_side(zb):
+        for h in others:
+            arrived(h, zb * cores + c, 2)
+            if cores > 1:
+                across(h, zb, 2).start()
+
+    def add(zb, i):
+        for h in others + [y]:
+            weights = wbuf[h, pl.ds(zb * cores, cores)].reshape(chunk, 3 * head)
+            acc[h, i] += jnp.dot(xbuf[i, zb], weights, preferred_element_type=jnp.float32)
+
+    def add_own(zb):
+        if cores > 1:
+            at = zb * cores + 1 - c
+            arrived(y, at, 0)
+            for h in others:
+                arrived(h, at, 1)
+                arrived(h, at, 2)
+        pltpu.make_async_copy(piece(zb), xbuf.at[x, zb], tsem.at[zb]).wait()
+        add(zb, x)
+
+    def add_other(zb):
+        for j in range(1, nx):
+            i = (x + j) % nx
+            pltpu.make_async_remote_copy(
+                src_ref=piece(zb), dst_ref=xbuf.at[i, zb],
+                send_sem=xsend.at[j - 1, zb], recv_sem=xrecv.at[i, zb],
+                device_id={"sp": (s + 1) % (nx * ny)}, device_id_type=MESH,
+            ).wait_recv()
+            add(zb, i)
 
     def own_rows(i):
         return pl.ds(pl.multiple_of(y * group + i * tok, tok), tok)
-
-    loads[3].wait()
-    qkv[own_rows(x), :] = project(x, y)
-
-    def from_side(zb):
-        for k in range(1, ny):
-            other = (y + ny - k) % ny
-            arrived(other, zb * cores + c)
-            if cores > 1:
-                across(other, zb).start()
-
-    from_side(z)
-    for t in range(1, nz):
-        pl.when(z - t >= 0)(lambda t=t: from_side(z - t))
-        pl.when(z + t < nz)(lambda t=t: from_side(z + t))
-    if cores > 1:
-        for k in range(1, ny):
-            for zb in range(nz):
-                arrived((y + k) % ny, zb * cores + 1 - c)
 
     def send_qkv(k, i):
         return pltpu.make_async_remote_copy(
             src_ref=qout.at[k - 1, i], dst_ref=qkv.at[own_rows(i)],
             send_sem=qsend.at[k - 1, i], recv_sem=qrecv.at[y, i],
-            device_id={"sp": ((y + k) % ny) * nx + x}, device_id_type=MESH,
+            device_id=aside(k), device_id_type=MESH,
         )
 
     def swap(i):
         for k in range(1, ny):
-            qout[k - 1, i] = project(i, (y + k) % ny)
+            qout[k - 1, i] = acc[others[k - 1], i].astype(jnp.bfloat16)
             send_qkv(k, i).start()
 
-    swap(x)
+    relay(0)
+    for t in range(nz):
+        if t + 1 < nz:
+            relay(t + 1)
+        step(t, from_side)
+        step(t, add_own)
+        if t == nz - 1:
+            swap(x)
+        step(t, add_other)
     for j in range(1, nx):
-        i = (x + j) % nx
-        pltpu.make_async_remote_copy(
-            src_ref=tok_hbm, dst_ref=xbuf.at[i],
-            send_sem=xsend.at[j - 1], recv_sem=xrecv.at[i],
-            device_id={"sp": (s + 1) % (nx * ny)}, device_id_type=MESH,
-        ).wait_recv()
-        swap(i)
-    for j in range(1, nx):
-        i = (x + j) % nx
-        qkv[own_rows(i), :] = project(i, y)
+        swap((x + j) % nx)
+    for i in range(nx):
+        qkv[own_rows(i), :] = acc[y, i].astype(jnp.bfloat16)
     for k in range(1, ny):
         other = (y + k) % ny
         for i in range(nx):
-            rows = pl.ds(pl.multiple_of(other * group + i * tok, tok), tok)
+            taken = pl.ds(pl.multiple_of(other * group + i * tok, tok), tok)
             pltpu.make_async_remote_copy(
-                src_ref=qout.at[k - 1, i], dst_ref=qkv.at[rows],
+                src_ref=qout.at[k - 1, i], dst_ref=qkv.at[taken],
                 send_sem=qsend.at[k - 1, i], recv_sem=qrecv.at[other, i],
                 device_id={"sp": other * nx + x}, device_id_type=MESH,
             ).wait_recv()
@@ -236,16 +301,25 @@
         ).wait_recv()
     out_ref[...] = obuf[...]
 
-    for j in range(1, nx):
-        send_tokens(j).wait_send()
     for zb in range(nz):
-        pl.when((z < nz - 1) & (zb <= z))(lambda zb=zb: up(zb).wait_send())
-        pl.when((z > 0) & (zb >= z))(lambda zb=zb: down(zb).wait_send())
+        for j in range(1, nx):
+            send_tokens(j, zb).wait_send()
+        upward = (z < nz - 1) & (zb <= z)
+        downward = (z > 0) & (zb >= z)
+        pl.when(upward)(lambda zb=zb: up(zb).wait_send())
+        pl.when(downward)(lambda zb=zb: down(zb).wait_send())
+        for h in others:
+            pl.when(upward)(lambda h=h, zb=zb: up_early(h, zb).wait_send())
+            pl.when(downward)(lambda h=h, zb=zb: down_early(h, zb).wait_send())
+            if cores > 1:
+                across(h, zb, 1).wait_send()
+                across(h, zb, 2).wait_send()
+        if cores > 1:
+            across(y, zb, 0).wait_send()
         for k in range(1, ny):
-            aside(k, zb).wait_send()
-        if cores > 1:
-            for h in range(ny):
-                across(h, zb).wait_send()
+            side_late(k, zb).wait_send()
+    for k in range(1, ny):
+        side_early(k).wait_send()
     for k in range(1, ny):
         for i in range(nx):
             send_qkv(k, i).wait_send()
@@ -270,21 +344,27 @@
         in_specs=[anywhere] * 4 + [vmem],
         out_specs=vmem,
         scratch_shapes=[
-            pltpu.VMEM((nx, tok, depth), jnp.bfloat16),
+            pltpu.VMEM((nx, nz, tok, cores * rows), jnp.bfloat16),
             pltpu.VMEM((ny, dp, rows, 3 * head), jnp.bfloat16),
+            pltpu.VMEM((ny, nx, tok, 3 * head), jnp.float32),
             pltpu.VMEM((length, 3 * head), jnp.bfloat16),
             pltpu.VMEM((ny - 1, nx, tok, 3 * head), jnp.bfloat16),
             pltpu.VMEM((length, 128), jnp.float32),
             pltpu.VMEM((length, head), jnp.bfloat16),
             pltpu.VMEM((tok, sp * head), jnp.bfloat16),
-            dma((4,)),
-            dma((nx - 1,)),
-            dma((nx,)),
-            dma((ny, dp)),
+            dma((3,)),
+            dma((nz,)),
+            dma((nx - 1, nz)),
+            dma((nx, nz)),
+            dma((2, ny, dp)),
             dma((nz,)),
             dma((nz,)),
             dma((ny, nz)),
+            dma((ny, nz)),
+            dma((ny, nz)),
+            dma((ny, nz)),
             dma((ny - 1, nz)),
+            dma((ny - 1,)),
             dma((ny - 1, nx)),
             dma((ny, nx)),
             dma((sp,)),

time: 59.3 us -> 60.7 us (1.024)
  Pallas kernels: 57.5 us -> 58.9 us
    pallas_call x1, Pallas kernels: 57.5 us -> 58.9 us  [body(): pl.pallas_call(functools.partial(kernel, nx, ny, nz, cores), out_shape=ja...]
where the time goes in v2:
time: 60.7 us; the launch traced here: 60.5 us
  Pallas kernels  58.9 us (97%)
  local copies, waits for them, and re-layouts  1.62 us (3%)
    pallas_call x1, Pallas kernels, body(): pl.pallas_call(functools.partial(kernel, nx, ny, nz, cores), out_shape=ja...  58.9 us
    unnamed x1, local copies, waits for them, and re-layouts  1.62 us

profile of v2, /device:TPU:0, one launch (start us, length us, event | category | flops | bytes accessed | tf_op | source)
XLA Modules:
  0.0 60.5 jit_solution(9711807906400947091)
XLA Ops:
  0.0 58.9 %shard_map.55 = bf16[192,512]{1,0:T(8,128)(2,1)} custom-call(bf16[192,4096]{1,0:T(8,128)(2,1)} %bitcast.3, bf16[512,128]{1,0:T(8,128)(2,1)} %wq_hbm.1, bf16[512,128]{1,0:T(8,128)(2,1)} %wk_hbm.1, bf16[512,128]{1,0:T(8,128)(2,1)} %wv_hbm.1, f32[1,768]{1,0:T(1,128)} %bitcast.5), custom_call_target="tpu_custom_call" | custom-call | tf_op jit(solution)/shard_map/pallas_call | solution.py:341
  58.9 1.6 %copy.7 = bf16[1,192,512]{2,1,0:T(8,128)(2,1)} copy(bf16[1,192,512]{2,1,0:T(8,128)(2,1)} %bitcast.4) | data formatting | bytes 393216

commit v3 on v2

--- a/solution.py
+++ b/solution.py
@@ -21,7 +21,7 @@
 ):
     tok, depth = tok_hbm.shape
     rows, head = wq_hbm.shape
-    early = rows // 4
+    early = rows // 16
     chunk = cores * rows
     group = nx * tok
     length = ny * group
@@ -299,7 +299,8 @@
             send_sem=osend.at[source], recv_sem=orecv.at[source],
             device_id={"sp": source}, device_id_type=MESH,
         ).wait_recv()
-    out_ref[...] = obuf[...]
+    last = pltpu.make_async_copy(obuf, out_ref, lsem.at[0])
+    last.start()
 
     for zb in range(nz):
         for j in range(1, nx):
@@ -325,6 +326,7 @@
             send_qkv(k, i).wait_send()
     for to in range(nx * ny):
         pl.when(s != to)(lambda to=to: send_out(to).wait_send())
+    last.wait()
 
 
 def body(sp, dp, tokens, query_weight, key_weight, value_weight, cum_gate):
@@ -342,7 +344,7 @@
         functools.partial(kernel, nx, ny, nz, cores),
         out_shape=jax.ShapeDtypeStruct((tok, sp * head), jnp.bfloat16),
         in_specs=[anywhere] * 4 + [vmem],
-        out_specs=vmem,
+        out_specs=anywhere,
         scratch_shapes=[
             pltpu.VMEM((nx, nz, tok, cores * rows), jnp.bfloat16),
             pltpu.VMEM((ny, dp, rows, 3 * head), jnp.bfloat16),

time: 60.7 us -> 59 us (0.972)
  Pallas kernels: 58.9 us -> 57.2 us
    pallas_call x1, Pallas kernels: 58.9 us -> 57.2 us  [body(): pl.pallas_call(functools.partial(kernel, nx, ny, nz, cores), out_shape=ja...]
where the time goes in v3:
time: 59 us; the launch traced here: 58.9 us
  Pallas kernels  57.2 us (97%)
  local copies, waits for them, and re-layouts  1.62 us (3%)
    pallas_call x1, Pallas kernels, body(): pl.pallas_call(functools.partial(kernel, nx, ny, nz, cores), out_shape=ja...  57.2 us
    unnamed x1, local copies, waits for them, and re-layouts  1.62 us

profile of v3, /device:TPU:0, one launch (start us, length us, event | category | flops | bytes accessed | tf_op | source)
XLA Modules:
  0.0 58.9 jit_solution(15668599234004367822)
XLA Ops:
  0.0 57.2 %shard_map.55 = bf16[192,512]{1,0:T(8,128)(2,1)} custom-call(bf16[192,4096]{1,0:T(8,128)(2,1)} %bitcast.3, bf16[512,128]{1,0:T(8,128)(2,1)} %wq_hbm.1, bf16[512,128]{1,0:T(8,128)(2,1)} %wk_hbm.1, bf16[512,128]{1,0:T(8,128)(2,1)} %wv_hbm.1, f32[1,768]{1,0:T(1,128)} %bitcast.5), custom_call_target="tpu_custom_call" | custom-call | tf_op jit(solution)/shard_map/pallas_call | solution.py:343
  57.2 1.6 %copy.7 = bf16[1,192,512]{2,1,0:T(8,128)(2,1)} copy(bf16[1,192,512]{2,1,0:T(8,128)(2,1)} %bitcast.4) | data formatting | bytes 393216

commit v4 on v3

--- a/solution.py
+++ b/solution.py
@@ -9,7 +9,7 @@
 from jax.sharding import PartitionSpec as P
 
 MESH = pl.DeviceIdType.MESH
-block_rows = 256
+block_rows = 128
 
 
 def kernel(

time: 59 us -> 59.2 us (level)
  no operation moved by 1% of the time
where the time goes in v4:
time: 59.2 us; the launch traced here: 59 us
  Pallas kernels  57.4 us (97%)
  local copies, waits for them, and re-layouts  1.62 us (3%)
    pallas_call x1, Pallas kernels, body(): pl.pallas_call(functools.partial(kernel, nx, ny, nz, cores), out_shape=ja...  57.4 us
    unnamed x1, local copies, waits for them, and re-layouts  1.62 us

profile of v4, /device:TPU:0, one launch (start us, length us, event | category | flops | bytes accessed | tf_op | source)
XLA Modules:
  0.0 59.0 jit_solution(11101996787721447182)
XLA Ops:
  0.0 57.4 %shard_map.55 = bf16[192,512]{1,0:T(8,128)(2,1)} custom-call(bf16[192,4096]{1,0:T(8,128)(2,1)} %bitcast.3, bf16[512,128]{1,0:T(8,128)(2,1)} %wq_hbm.1, bf16[512,128]{1,0:T(8,128)(2,1)} %wk_hbm.1, bf16[512,128]{1,0:T(8,128)(2,1)} %wv_hbm.1, f32[1,768]{1,0:T(1,128)} %bitcast.5), custom_call_target="tpu_custom_call" | custom-call | tf_op jit(solution)/shard_map/pallas_call | solution.py:343
  57.4 1.6 %copy.7 = bf16[1,192,512]{2,1,0:T(8,128)(2,1)} copy(bf16[1,192,512]{2,1,0:T(8,128)(2,1)} %bitcast.4) | data formatting | bytes 393216
